TPU v7x, 32 devices: a whole 2x2x4 slice. The times are simulated.
32 devices in a mesh: sp: 8 (over z, x), tp: 4 (over y, core).
Axes of the slice: x: 2, y: 2, z: 4, core: 2. Of those that a mesh axis runs over, the one named last changes fastest.
Arguments:
- queries: bfloat16 [3072, 768], P('sp', 'tp'), may hold values from -8 to 8
- keys: bfloat16 [3072, 256], P('sp', 'tp'), may hold values from -8 to 8
- values: bfloat16 [3072, 256], P('sp', 'tp'), may hold values from -6 to 6
- sinks: float32 [12], P('tp'), may hold values from 1 to 6
- residual: bfloat16 [3072, 2048], P('sp'), may hold values from -6 to 6
- out_weight: bfloat16 [768, 2048], replicated, may hold values from -3 to 3
- norm_gain: float32 [2048], replicated, may hold values from 0.1 to 1.9
- shared_gate: bfloat16 [2048, 512], P(None, 'tp'), may hold values from -0.125 to 0.125
- shared_up: bfloat16 [2048, 512], P(None, 'tp'), may hold values from -0.125 to 0.125
- shared_down: bfloat16 [512, 2048], P('tp'), may hold values from -0.25 to 0.25
- expert_ids: int32 [3072, 2], P('sp'), may hold values from 0 to 15, all different within a row; in each aligned block of 96 rows (0 to 95, 96 to 191, ...) at most 24 rows name the same one
- route_weights: float32 [3072, 2], P(('sp', 'tp')), may hold values from 0.2 to 2
- expert_gate: bfloat16 [16, 2048, 1024], P('sp', None, 'tp'), may hold values from -0.125 to 0.125
- expert_up: bfloat16 [16, 2048, 1024], P('sp', None, 'tp'), may hold values from -0.125 to 0.125
- expert_down: bfloat16 [16, 1024, 2048], P('sp', 'tp'), may hold values from -0.1875 to 0.1875
Outputs:
- layer_out: bfloat16 [3072, 2048], P(('sp', 'tp'))
Inputs may be any that keep to these rules, and one draw needn't show every extreme that they name: `expert_ids`: each row names 2 different experts. In each aligned block of 96 rows no expert is named more than 24 times, a bound that some blocks reach.
All inputs are finite; a program needn't handle non-finite values.
Results may differ from a plain program's by a relative error of at most 0.018.
Values may be sent and summed in bfloat16 or wider, within the bound.
A program may use at most 128 MiB of HBM per device.

v0:
```python
import jax
import jax.numpy as jnp
from jax import lax
from jax.sharding import PartitionSpec as P

HEAD_DIM = 64
WINDOW = 128
GRID_W = 64
TOPK = 2


ROPE_BASE = 10000.0
NEG_LARGE = -1e30
NORM_EPSILON = 1e-06


def extended(x, sides, width):
    for axis, dim in sides:
        size, length = (lax.axis_size(axis), x.shape[dim])
        up = [(i, (i + 1) % size) for i in range(size - 1)]
        down = [(j, i) for i, j in up]
        last = lax.slice_in_dim(x, length - width, length, axis=dim)
        initial = lax.slice_in_dim(x, 0, width, axis=dim)
        before = lax.ppermute(last, axis, up)
        after = lax.ppermute(initial, axis, down)
        x = jnp.concatenate([before, x, after], axis=dim)
    return x


def rotary_turn(values, places, turn_sign):
    halfway = values.shape[-1] // 2
    quarter = halfway // 2
    spectrum = ROPE_BASE ** (-jnp.arange(0, halfway, 2, dtype=jnp.float32) / halfway)

    def rotate_by(segment, offsets_at):
        angles = turn_sign * offsets_at.astype(jnp.float32)[:, None] * spectrum[None, :]
        cosine = jnp.cos(angles)[:, None, :]
        sine_part = jnp.sin(angles)[:, None, :]
        former = segment[..., :quarter]
        latter = segment[..., quarter:]
        return jnp.concatenate(
            [former * cosine - latter * sine_part, former * sine_part + latter * cosine], axis=-1
        )

    return jnp.concatenate(
        [
            rotate_by(values[..., :halfway], places // GRID_W),
            rotate_by(values[..., halfway:], places % GRID_W),
        ],
        axis=-1,
    )


def gated_hidden(gathered_rows, gate_weight, up_weight):
    gate_values = jnp.dot(gathered_rows, gate_weight, preferred_element_type=jnp.float32)
    up_values = jnp.dot(gathered_rows, up_weight, preferred_element_type=jnp.float32)
    return (jax.nn.silu(gate_values) * up_values).astype(jnp.bfloat16)


def per_device(
    queries,
    keys,
    values,
    sinks,
    residual,
    out_weight,
    norm_gain,
    shared_gate,
    shared_up,
    shared_down,
    expert_ids,
    route_weights,
    expert_gate,
    expert_up,
    expert_down,
):
    block_rows = queries.shape[0]
    width_split = lax.axis_size("tp")
    token_split = lax.axis_size("sp")
    width_index = lax.axis_index("tp")
    key_heads = keys.shape[1] // HEAD_DIM
    heads_local = queries.shape[1] // HEAD_DIM
    group_size = heads_local // key_heads
    first_row = lax.axis_index("sp") * block_rows
    total_rows = token_split * block_rows
    places = first_row + jnp.arange(block_rows, dtype=jnp.int32)
    turned_queries = rotary_turn(
        queries.astype(jnp.float32).reshape(block_rows, heads_local, HEAD_DIM), places, 1.0
    ).astype(jnp.bfloat16)
    turned_keys = rotary_turn(
        keys.astype(jnp.float32).reshape(block_rows, key_heads, HEAD_DIM), places, 1.0
    ).astype(jnp.bfloat16)
    joined = jnp.concatenate(
        [turned_keys.reshape(block_rows, key_heads * HEAD_DIM), values], axis=1
    )
    widened = extended(joined, (("sp", 0),), WINDOW)
    blocks = block_rows // WINDOW
    windows = jnp.concatenate(
        [
            widened[shift_index * WINDOW : shift_index * WINDOW + blocks * WINDOW].reshape(
                blocks, WINDOW, -1
            )
            for shift_index in range(3)
        ],
        axis=1,
    )
    key_win = windows[..., : key_heads * HEAD_DIM].reshape(blocks, 3 * WINDOW, key_heads, HEAD_DIM)
    value_win = windows[..., key_heads * HEAD_DIM :].reshape(
        blocks, 3 * WINDOW, key_heads, HEAD_DIM
    )
    query_blocks = turned_queries.reshape(blocks, WINDOW, key_heads, group_size, HEAD_DIM)
    scores = jnp.einsum(
        "bqkgd,bmkd->bkgqm", query_blocks, key_win, preferred_element_type=jnp.float32
    ) * HEAD_DIM ** (-0.5)
    block_first = first_row + jnp.arange(blocks, dtype=jnp.int32) * WINDOW
    query_at = block_first[:, None, None] + jnp.arange(WINDOW, dtype=jnp.int32)[None, :, None]
    key_at = (
        block_first[:, None, None] - WINDOW + jnp.arange(3 * WINDOW, dtype=jnp.int32)[None, None, :]
    )
    allowed = (jnp.abs(query_at - key_at) <= WINDOW) & (key_at >= 0) & (key_at < total_rows)
    scores = jnp.where(allowed[:, None, None], scores, NEG_LARGE)
    sink_logit = sinks.reshape(key_heads, group_size)[None, :, :, None, None]
    highest = jnp.maximum(jnp.max(scores, axis=-1, keepdims=True), sink_logit)
    lifted = jnp.exp(scores - highest)
    denominator = jnp.sum(lifted, axis=-1, keepdims=True) + jnp.exp(sink_logit - highest)
    probabilities = (lifted / denominator).astype(jnp.bfloat16)
    attended = jnp.einsum(
        "bkgqm,bmkd->bqkgd", probabilities, value_win, preferred_element_type=jnp.float32
    )
    attended = attended.astype(jnp.bfloat16).reshape(block_rows, heads_local * HEAD_DIM)
    model_width = out_weight.shape[1]
    projected = jnp.dot(
        lax.all_gather(attended, "tp", axis=1, tiled=True),
        out_weight,
        preferred_element_type=jnp.float32,
    )
    mixed_rows = (residual.astype(jnp.float32) + projected).astype(jnp.bfloat16)
    mixed_float = mixed_rows.astype(jnp.float32)
    scale_rows = lax.rsqrt(
        jnp.mean(mixed_float * mixed_float, axis=-1, keepdims=True) + NORM_EPSILON
    )
    normed = (mixed_float * scale_rows * norm_gain).astype(jnp.bfloat16)
    own_rows = block_rows // width_split
    shared_hidden = gated_hidden(normed, shared_gate, shared_up)
    shared_part = jnp.dot(shared_hidden, shared_down, preferred_element_type=jnp.float32)
    shared_part = shared_part.astype(jnp.bfloat16).reshape(width_split, own_rows, model_width)
    experts_here = expert_gate.shape[0]
    experts_all = experts_here * token_split
    capacity = max(2, 2 * own_rows * TOPK // experts_all)
    normed_pad = jnp.concatenate([normed, jnp.zeros((1, model_width), jnp.bfloat16)], axis=0)
    own_routes = lax.dynamic_slice_in_dim(expert_ids, width_index * own_rows, own_rows, 0).reshape(
        1, own_rows * TOPK
    )
    owner_count = own_routes.shape[0]
    assigns = own_routes.shape[1]
    order_index = jnp.arange(assigns, dtype=jnp.int32)
    matches = (own_routes[:, :, None] == own_routes[:, None, :]) & (
        order_index[None, None, :] < order_index[None, :, None]
    )
    rank_in_block = jnp.sum(matches.astype(jnp.int32), axis=2)
    slot_index = own_routes * capacity + rank_in_block
    owner_index = jnp.arange(owner_count, dtype=jnp.int32)[:, None]
    token_of = (width_index + owner_index) * own_rows + order_index[None, :] // TOPK
    slot_token = (
        jnp.full((owner_count, experts_all * capacity), block_rows, jnp.int32)
        .at[owner_index, slot_index]
        .set(token_of)
    )
    slot_single, slot_token = (slot_index, slot_token)
    outgoing = normed_pad[slot_token].reshape(1, token_split, experts_here, capacity, model_width)
    arrived = lax.all_to_all(outgoing, "sp", split_axis=1, concat_axis=1, tiled=True)
    slot_batch = lax.all_gather(arrived, "tp", axis=0, tiled=True)
    gate_values = jnp.einsum(
        "osecd,edh->osech", slot_batch, expert_gate, preferred_element_type=jnp.float32
    )
    up_values = jnp.einsum(
        "osecd,edh->osech", slot_batch, expert_up, preferred_element_type=jnp.float32
    )
    hidden = (jax.nn.silu(gate_values) * up_values).astype(jnp.bfloat16)
    partial_value = jnp.einsum(
        "osech,ehd->osecd", hidden, expert_down, preferred_element_type=jnp.float32
    ).astype(jnp.bfloat16)
    own_slots = slot_single[0]
    summed, shared_sum = (
        lax.psum_scatter(partial_value, "tp", scatter_dimension=0, tiled=True).astype(jnp.float32),
        lax.psum_scatter(shared_part, "tp", scatter_dimension=0, tiled=True).astype(jnp.float32),
    )
    returned = lax.all_to_all(
        summed.astype(jnp.bfloat16), "sp", split_axis=1, concat_axis=1, tiled=True
    )
    flat_back = returned.reshape(experts_all * capacity, model_width)
    picked = flat_back[own_slots].astype(jnp.float32).reshape(own_rows, TOPK, model_width)
    routed = jnp.sum(route_weights[:, :, None] * picked, axis=1)
    mixed_own = lax.dynamic_slice_in_dim(mixed_float, width_index * own_rows, own_rows, 0)
    return (mixed_own + shared_sum[0] + routed).astype(jnp.bfloat16)


def solution(mesh):
    placed = (
        P("sp", "tp"),
        P("sp", "tp"),
        P("sp", "tp"),
        P("tp"),
        P("sp", None),
        P(),
        P(),
        P(None, "tp"),
        P(None, "tp"),
        P("tp", None),
        P("sp", None),
        P(("sp", "tp"), None),
        P("sp", None, "tp"),
        P("sp", None, "tp"),
        P("sp", "tp", None),
    )
    return jax.shard_map(
        per_device, mesh=mesh, in_specs=placed, out_specs=P(("sp", "tp"), None), check_vma=False
    )
```

profile of v0, /device:TPU:0, one launch (start us, length us, event | category | flops | bytes accessed | tf_op | source)
XLA Modules:
  0.0 352.5 jit_solution(5374777021530814366)
XLA Ops:
  6.6 1.0 bitcast_convert_fusion
  9.0 1.5 copy.99
  10.6 1.2 concatenate.67
  12.4 5.5 %collective-permute-start = (bf16[128,128]{1,0:T(8,128)(2,1)}, bf16[128,128]{1,0:T(8,128)(2,1)}, u32[]{:S(2)}, u32[]{:S(2)}) collective-permute-start(bf16[128,128]{1,0:T(8,128)(2,1)} %get-tuple-element.21), channel_id=1, source_target_pairs={{0,4},{4,8},{8,12},{12,16},{16,20},{20,24},{24,28},{1,5},{5,9},{9,... | collective-permute-start | bytes 98312 | tf_op jit(solution)/shard_map/ppermute | solution.py:24
  17.8 1.3 collective-permute-start.1
  25.8 1.2 scatter_custom_fusion
  28.6 1.0 convert.53
  29.6 2.4 fusion.22
  35.0 0.9 pad_maximum_fusion
  35.9 1.5 fusion.72
  38.4 7.6 %all_gather.6 = bf16[384,768]{0,1:T(8,128)(2,1)S(1)} all-gather(bf16[384,192]{0,1:T(8,128)(2,1)S(1)} %bitcast.153), channel_id=1, replica_groups=mesh['sp'=8,'tp'=4] {'tp'}, dimensions={1}, use_global_device_ids=true | all-gather | bytes 737280 | tf_op jit(solution)/shard_map/all_gather | solution.py:133
  46.0 1.8 multiply_reduce_fusion
  48.1 1.3 copy-done.2
  49.4 1.1 copy-done.1
  50.5 1.3 concatenate.82
  51.8 6.7 %gather_fusion = bf16[384,2048]{1,0:T(8,128)(2,1)} fusion(bf16[385,2048]{1,0:T(8,128)(2,1)} %concatenate.82, s32[1024]{0:T(1024)S(1)} %pad_clamp_fusion.1), kind=kCustom, calls=%fused_computation | custom fusion | bytes 3147264 | tf_op jit(solution)/shard_map/gather | solution.py:170
  58.5 44.4 %all_to_all.10 = bf16[1,8,2,24,2048]{4,3,0,2,1:T(8,128)(2,1)S(1)} all-to-all(bf16[1,8,2,24,2048]{4,3,0,2,1:T(8,128)(2,1)} %bitcast.151), channel_id=1, replica_groups=mesh['sp'=8,'tp'=4] {'sp'}, dimensions={1} | all-to-all | bytes 3145728 | tf_op jit(solution)/shard_map/all_to_all | solution.py:171
  102.9 1.3 copy.117
  104.5 44.5 %all-gather.2.cloned.1.call-done = bf16[4,8,2,24,2048]{4,3,1,0,2:T(8,128)(2,1)} async-done(((bf16[1,8,2,24,2048]{4,3,1,0,2:T(8,128)(2,1)}), bf16[4,8,2,24,2048]{4,3,1,0,2:T(8,128)(2,1)}) %all-gather.2.cloned.1.call-update) | async-done | bytes 6291472 | tf_op jit(solution)/shard_map/all_gather | solution.py:172
  148.9 6.4 %fusion.4 = f32[2,4,8,24,256]{4,3,2,1,0:T(8,128)} fusion(bf16[4,8,2,24,2048]{4,3,1,0,2:T(8,128)(2,1)} %all-gather.2.cloned.1.call-done, bf16[2,2048,256]{2,1,0:T(8,128)(2,1)} %param.27), kind=kOutput, calls=%fused_computation.12 | convolution fusion | flops 1610612736 | bytes 9961472 | tf_op jit(solution)/shard_map/osecd,edh->osech/dot_general | solution.py:173
  155.3 10.7 %convert_bitcast_fusion = bf16[4,8,2,24,2048]{4,3,1,0,2:T(8,128)(2,1)} fusion(bf16[2,256,2048]{2,1,0:T(8,128)(2,1)} %param.29, f32[2,4,8,24,256]{4,3,2,1,0:T(8,128)} %fusion.4, bf16[4,8,2,24,2048]{4,3,1,0,2:T(8,128)(2,1)} %all-gather.2.cloned.1.call-done, bf16[2,2048,256]{2,1,0:T(8,128)(2,1)} %param.28), kind=kOutput, calls=%fused_computation.3 | convolution fusion | flops 3226730496 | bytes 18350080 | tf_op jit(solution)/shard_map/osech,ehd->osecd/dot_general | solution.py:180
  167.3 2.1 fusion.73
  169.4 4.6 %convolution_convert_fusion = bf16[384,2048]{1,0:T(8,128)(2,1)} fusion(bf16[128,2048]{1,0:T(8,128)(2,1)} %param.24, bf16[384,2048]{1,0:T(8,128)(2,1)} %copy-done.1, bf16[2048,128]{1,0:T(8,128)(2,1)} %param.23, f32[384,128]{1,0:T(8,128)S(1)} %fusion.73), kind=kOutput, calls=%fused_computation.7 | convolution fusion | flops 403734528 | bytes 4390912 | tf_op jit(solution)/shard_map/dot_general | solution.py:145
  174.1 111.8 %all-reduce.5.cloned.1.call-done = bf16[4,8,2,24,2048]{4,3,1,0,2:T(8,128)(2,1)} async-done(((bf16[4,8,2,24,2048]{4,3,1,0,2:T(8,128)(2,1)}), bf16[4,8,2,24,2048]{4,3,1,0,2:T(8,128)(2,1)}) %all-reduce.5.cloned.1.call-update) | async-done | bytes 6291472
  285.8 2.2 constant_dynamic-slice_fusion
  288.0 1.3 copy.118
  289.4 5.6 %all-to-all-start.1 = ((bf16[1,8,2,24,2048]{4,3,0,2,1:T(8,128)(2,1)}), bf16[1,8,2,24,2048]{4,3,0,2,1:T(8,128)(2,1)}, u32[]{:S(2)}, u32[]{:S(2)}) async-start(bf16[1,8,2,24,2048]{4,3,0,2,1:T(8,128)(2,1)} %copy.118), calls=%async_computation.2 | async-start | bytes 3145728 | tf_op jit(solution)/shard_map/all_to_all | solution.py:188
  295.3 36.4 %all-to-all-done.1 = bf16[1,8,2,24,2048]{4,3,0,2,1:T(8,128)(2,1)} async-done(((bf16[1,8,2,24,2048]{4,3,0,2,1:T(8,128)(2,1)}), bf16[1,8,2,24,2048]{4,3,0,2,1:T(8,128)(2,1)}, u32[]{:S(2)}, u32[]{:S(2)}) %all-to-all-start.1) | async-done | bytes 1572896 | tf_op jit(solution)/shard_map/all_to_all | solution.py:188
  331.7 4.4 %gather_fusion.1 = bf16[192,2048]{1,0:T(8,128)(2,1)} fusion(bf16[384,2048]{1,0:T(8,128)(2,1)} %bitcast.36, s32[1024]{0:T(1024)S(1)} %pad_clamp_fusion), kind=kCustom, calls=%fused_computation.1 | custom fusion | bytes 1573632 | tf_op jit(solution)/shard_map/gather | solution.py:192
  336.1 2.9 reshape.713
  339.0 4.6 %multiply_reduce_fusion.1 = f32[96,2048]{1,0:T(8,128)} fusion(f32[96,2,2048]{2,1,0:T(2,128)} %reshape.713, f32[96,2]{1,0:T(8,128)S(1)} %copy.113), kind=kLoop, calls=%fused_computation.24 | loop fusion | flops 589824 | bytes 2360064 | tf_op jit(solution)/shard_map/reduce_sum | solution.py:193
  343.7 2.3 fusion.19
  (90 shorter events, 16.3 us)
Async XLA Ops:
  6.5 39.4 %copy-start = (bf16[768,2048]{1,0:T(8,128)(2,1)S(1)}, bf16[768,2048]{1,0:T(8,128)(2,1)}, u32[]{:S(2)}) copy-start(bf16[768,2048]{1,0:T(8,128)(2,1)} %param.20) | copy-start | bytes 9437188
  6.5 142.4 %all-gather.2.cloned.1.call-start = ((), (), s32[]{:S(2)}) async-start(), calls=%async_computation.4 | async-start | bytes 7864320 | tf_op jit(solution)/shard_map/all_gather | solution.py:172
  6.6 2.5 copy-start.10
  6.6 2.4 copy-start.8
  7.8 1.2 copy-start.5
  7.8 1.2 copy-start.6
  7.8 1.2 copy-start.7
  12.4 21.5 %collective-permute-start = (bf16[128,128]{1,0:T(8,128)(2,1)}, bf16[128,128]{1,0:T(8,128)(2,1)}, u32[]{:S(2)}, u32[]{:S(2)}) collective-permute-start(bf16[128,128]{1,0:T(8,128)(2,1)} %get-tuple-element.21), channel_id=1, source_target_pairs={{0,4},{4,8},{8,12},{12,16},{16,20},{20,24},{24,28},{1,5},{5,9},{9,... | collective-permute-start | bytes 98312 | tf_op jit(solution)/shard_map/ppermute | solution.py:24
  17.8 16.1 %collective-permute-start.1 = (bf16[128,128]{1,0:T(8,128)(2,1)}, bf16[128,128]{1,0:T(8,128)(2,1)}, u32[]{:S(2)}, u32[]{:S(2)}) collective-permute-start(bf16[128,128]{1,0:T(8,128)(2,1)} %get-tuple-element.22), channel_id=1, source_target_pairs={{4,0},{8,4},{12,8},{16,12},{20,16},{24,20},{28,24},{5,1},{9,5},{13... | collective-permute-start | bytes 98312 | tf_op jit(solution)/shard_map/ppermute | solution.py:25
  28.6 3.4 copy-start.4
  34.7 2.7 copy-start.11
  37.8 8.2 %copy-start.3 = (bf16[384,2048]{1,0:T(8,128)(2,1)S(1)}, bf16[384,2048]{1,0:T(8,128)(2,1)}, u32[]{:S(2)}) copy-start(bf16[384,2048]{1,0:T(8,128)(2,1)} %param.19) | copy-start | bytes 4718596
  46.0 1.8 copy-start.9
  47.7 1.6 copy-start.2
  49.4 1.1 copy-start.1
  104.2 181.6 %all-reduce.5.cloned.1.call-start = ((), (), s32[]{:S(2)}) async-start(), calls=%async_computation.5 | async-start | bytes 12582912
  166.1 0.7 copy-start.13
  166.1 177.6 %reduce-scatter.5.cloned.1.call-start = ((), (), s32[]{:S(2)}) async-start(), calls=%async_computation.3 | async-start | bytes 1966080 | tf_op jit(solution)/shard_map/reduce_scatter | solution.py:186
  289.4 5.8 %copy-start.12 = (f32[96,2]{0,1:T(2,128)S(1)}, f32[96,2]{0,1:T(2,128)}, u32[]{:S(2)}) copy-start(f32[96,2]{0,1:T(2,128)} %param.26) | copy-start | bytes 2308
  289.4 42.4 %all-to-all-start.1 = ((bf16[1,8,2,24,2048]{4,3,0,2,1:T(8,128)(2,1)}), bf16[1,8,2,24,2048]{4,3,0,2,1:T(8,128)(2,1)}, u32[]{:S(2)}, u32[]{:S(2)}) async-start(bf16[1,8,2,24,2048]{4,3,0,2,1:T(8,128)(2,1)} %copy.118), calls=%async_computation.2 | async-start | bytes 3145728 | tf_op jit(solution)/shard_map/all_to_all | solution.py:188
Sparse Core Ops, SparseCore 0:
  104.3 44.5 all-gather.1
  166.2 119.5 all-reduce.4
  288.4 28.2 reduce-scatter.4
where the time goes:
time: 354 us; the launch traced here: 353 us
  waiting for transfers between devices  193 us (55%)
  blocking collectives  52 us (15%)
  local copies, waits for them, and re-layouts  36.7 us (10%)
  matrix products  27.5 us (8%)
  other arithmetic  17.4 us (5%)
  between operations  13.4 us (4%)
  starting transfers between devices  12.7 us (4%)
    unnamed x4, waiting for transfers between devices  112 us
    all_gather x1, waiting for transfers between devices, per_device(): slot_batch = lax.all_gather(arrived, 'tp', axis=0, tiled=True)  44.5 us
    all_to_all x1, blocking collectives, per_device(): lax.all_to_all(outgoing, 'sp', split_axis=1, concat_axis=1, tiled=True)  44.4 us
    all_to_all x1, waiting for transfers between devices, per_device(): lax.all_to_all(summed.astype(jnp.bfloat16), 'sp', split_axis=1, concat_ax...  36.4 us
    dot_general x1, matrix products, per_device(): jnp.einsum('osech,ehd->osecd', hidden, expert_down, preferred_element_typ...  10.7 us
    unnamed x37, local copies, waits for them, and re-layouts  8.2 us
    all_gather x1, blocking collectives, per_device(): lax.all_gather(attended, 'tp', axis=1, tiled=True)  7.55 us
  transfers between devices with their start and end apart: 6, of which 3 were waited for; matrix products, arithmetic and copies ran while one was open for 11% of the time, Pallas kernels for 0%

commit v1 on v0

--- a/solution.py
+++ b/solution.py
@@ -1,7 +1,14 @@
 import jax
 import jax.numpy as jnp
 from jax import lax
+from jax.experimental import pallas as pl
+from jax.experimental.pallas import tpu as pltpu
 from jax.sharding import PartitionSpec as P
+import functools
+
+MESH = pl.DeviceIdType.MESH
+VMEM = pl.BlockSpec(memory_space=pltpu.VMEM)
+VMEM_LIMIT = 60 * 1024 * 1024
 
 HEAD_DIM = 64
 WINDOW = 128
@@ -55,6 +62,263 @@
     gate_values = jnp.dot(gathered_rows, gate_weight, preferred_element_type=jnp.float32)
     up_values = jnp.dot(gathered_rows, up_weight, preferred_element_type=jnp.float32)
     return (jax.nn.silu(gate_values) * up_values).astype(jnp.bfloat16)
+
+
+def places_of(token_split, width_split):
+    sp_at = lax.axis_index("sp")
+    tp_at = lax.axis_index("tp")
+    pair = tp_at + 1 - 2 * (tp_at % 2)
+    cross = (tp_at + width_split // 2) % width_split
+    return sp_at, tp_at, pair, cross
+
+
+def greet(token_split, sp_at, tp_at, pair, cross):
+    barrier = pltpu.get_barrier_semaphore()
+
+    @pl.loop(1, token_split)
+    def _(i):
+        pl.semaphore_signal(
+            barrier, inc=1, device_id=((sp_at + i) % token_split, tp_at), device_id_type=MESH
+        )
+
+    for partner in (pair, cross):
+        pl.semaphore_signal(barrier, inc=1, device_id=(sp_at, partner), device_id_type=MESH)
+    pl.semaphore_wait(barrier, token_split + 1)
+
+
+def dispatch_kernel(token_split, width_split, rows_ref, out_ref, local_sem, send, recv):
+    sp_at, tp_at, pair, cross = places_of(token_split, width_split)
+    greet(token_split, sp_at, tp_at, pair, cross)
+
+    def remote(stage, i, source, target, where):
+        return pltpu.make_async_remote_copy(
+            src_ref=source,
+            dst_ref=target,
+            send_sem=send.at[stage, i],
+            recv_sem=recv.at[stage, i],
+            device_id=where,
+            device_id_type=MESH,
+        )
+
+    def along(i):
+        there = (sp_at + i) % token_split
+        return remote(0, i, rows_ref.at[there], out_ref.at[:, tp_at, sp_at], (there, tp_at))
+
+    def passed(stage, i, block, partner):
+        piece = out_ref.at[:, block, (sp_at + token_split - i) % token_split]
+        return remote(stage, i, piece, piece, (sp_at, partner))
+
+    @pl.loop(1, token_split)
+    def _(i):
+        along(i).start()
+
+    own = pltpu.make_async_copy(rows_ref.at[sp_at], out_ref.at[:, tp_at, sp_at], local_sem)
+    own.start()
+    own.wait()
+    passed(1, 0, tp_at, cross).start()
+    passed(2, 0, tp_at, pair).start()
+
+    @pl.loop(1, token_split)
+    def _(i):
+        along(i).wait_recv()
+        passed(1, i, tp_at, cross).start()
+        passed(2, i, tp_at, pair).start()
+
+    @pl.loop(0, token_split)
+    def _(i):
+        passed(1, i, tp_at, cross).wait_recv()
+        passed(3, i, cross, pair).start()
+
+    @pl.loop(0, token_split)
+    def _(i):
+        passed(2, i, tp_at, pair).wait()
+        passed(1, i, tp_at, cross).wait_send()
+        passed(3, i, cross, pair).wait()
+
+    @pl.loop(1, token_split)
+    def _(i):
+        along(i).wait_send()
+
+
+def dispatch(rows, token_split, width_split):
+    _, experts, cap, width = rows.shape
+    return pl.pallas_call(
+        functools.partial(dispatch_kernel, token_split, width_split),
+        out_shape=jax.ShapeDtypeStruct(
+            (experts, width_split, token_split, cap, width), rows.dtype
+        ),
+        in_specs=[VMEM],
+        out_specs=VMEM,
+        scratch_shapes=[
+            pltpu.SemaphoreType.DMA,
+            pltpu.SemaphoreType.DMA((4, token_split)),
+            pltpu.SemaphoreType.DMA((4, token_split)),
+        ],
+        compiler_params=pltpu.CompilerParams(
+            collective_id=1, has_side_effects=True, vmem_limit_bytes=VMEM_LIMIT
+        ),
+        name="dispatch",
+    )(rows)
+
+
+def collect_kernel(
+    token_split,
+    width_split,
+    part_ref,
+    shared_ref,
+    back_ref,
+    shared_out,
+    from_pair,
+    to_cross,
+    from_cross,
+    final,
+    shared_pair,
+    shared_cross,
+    shared_got,
+    send,
+    recv,
+    shared_send,
+    shared_recv,
+):
+    sp_at, tp_at, pair, cross = places_of(token_split, width_split)
+    pair_cross = (pair + width_split // 2) % width_split
+    greet(token_split, sp_at, tp_at, pair, cross)
+
+    def copy(source, target, sems, where):
+        return pltpu.make_async_remote_copy(
+            src_ref=source,
+            dst_ref=target,
+            send_sem=sems[0],
+            recv_sem=sems[1],
+            device_id=where,
+            device_id_type=MESH,
+        )
+
+    def at(stage, i):
+        return send.at[stage, i], recv.at[stage, i]
+
+    def at_shared(stage):
+        return shared_send.at[stage], shared_recv.at[stage]
+
+    def place(i):
+        return (sp_at + 1 + i) % token_split
+
+    def pair_copy(side, i):
+        block = pair_cross if side == 0 else pair
+        there = place(i)
+        return copy(
+            part_ref.at[:, block, there], from_pair.at[side, there], at(side, i), (sp_at, pair)
+        )
+
+    def cross_copy(i):
+        there = place(i)
+        return copy(to_cross.at[there], from_cross.at[there], at(2, i), (sp_at, cross))
+
+    def along_copy(i):
+        there = place(i)
+        return copy(final.at[there], back_ref.at[sp_at], at(3, i), (there, tp_at))
+
+    def shared_copy(side):
+        block = pair_cross if side == 0 else pair
+        return copy(shared_ref.at[block], shared_pair.at[side], at_shared(side), (sp_at, pair))
+
+    shared_over = copy(shared_cross, shared_got, at_shared(2), (sp_at, cross))
+
+    @pl.loop(0, token_split)
+    def _(i):
+        pair_copy(0, i).start()
+
+    shared_copy(0).start()
+
+    @pl.loop(0, token_split)
+    def _(i):
+        pair_copy(1, i).start()
+
+    shared_copy(1).start()
+
+    def total(*terms):
+        value = terms[0].astype(jnp.float32)
+        for term in terms[1:]:
+            value = value + term.astype(jnp.float32)
+        return value
+
+    @pl.loop(0, token_split)
+    def _(i):
+        there = place(i)
+        pair_copy(0, i).wait_recv()
+        to_cross[there] = total(part_ref[:, cross, there], from_pair[0, there]).astype(
+            to_cross.dtype
+        )
+        cross_copy(i).start()
+
+    shared_copy(0).wait_recv()
+    shared_cross[...] = total(shared_ref[cross], shared_pair[0]).astype(shared_cross.dtype)
+    shared_over.start()
+
+    def summed(i):
+        there = place(i)
+        pair_copy(1, i).wait_recv()
+        cross_copy(i).wait_recv()
+        return total(part_ref[:, tp_at, there], from_pair[1, there], from_cross[there]).astype(
+            back_ref.dtype
+        )
+
+    @pl.loop(0, token_split - 1)
+    def _(i):
+        final[place(i)] = summed(i)
+        along_copy(i).start()
+
+    back_ref[sp_at] = summed(token_split - 1)
+    shared_copy(1).wait_recv()
+    shared_over.wait_recv()
+    shared_out[...] = total(shared_ref[tp_at], shared_pair[1], shared_got[...])
+
+    @pl.loop(0, token_split)
+    def _(i):
+        pair_copy(0, i).wait_send()
+        pair_copy(1, i).wait_send()
+        cross_copy(i).wait_send()
+
+    shared_copy(0).wait_send()
+    shared_copy(1).wait_send()
+    shared_over.wait_send()
+
+    @pl.loop(0, token_split - 1)
+    def _(i):
+        along_copy(i).wait()
+
+
+def collect(part, shared, token_split, width_split):
+    experts, _, _, cap, width = part.shape
+    own = shared.shape[1]
+    block = (token_split, experts, cap, width)
+    kind = part.dtype
+    return pl.pallas_call(
+        functools.partial(collect_kernel, token_split, width_split),
+        out_shape=(
+            jax.ShapeDtypeStruct(block, kind),
+            jax.ShapeDtypeStruct((own, width), jnp.float32),
+        ),
+        in_specs=[VMEM] * 2,
+        out_specs=(VMEM, VMEM),
+        scratch_shapes=[
+            pltpu.VMEM((2,) + block, kind),
+            pltpu.VMEM(block, kind),
+            pltpu.VMEM(block, kind),
+            pltpu.VMEM(block, kind),
+            pltpu.VMEM((2, own, width), kind),
+            pltpu.VMEM((own, width), kind),
+            pltpu.VMEM((own, width), kind),
+            pltpu.SemaphoreType.DMA((4, token_split)),
+            pltpu.SemaphoreType.DMA((4, token_split)),
+            pltpu.SemaphoreType.DMA((3,)),
+            pltpu.SemaphoreType.DMA((3,)),
+        ],
+        compiler_params=pltpu.CompilerParams(
+            collective_id=2, has_side_effects=True, vmem_limit_bytes=VMEM_LIMIT
+        ),
+        name="collect",
+    )(part, shared)
 
 
 def per_device(
@@ -147,52 +411,48 @@
     experts_here = expert_gate.shape[0]
     experts_all = experts_here * token_split
     capacity = max(2, 2 * own_rows * TOPK // experts_all)
-    normed_pad = jnp.concatenate([normed, jnp.zeros((1, model_width), jnp.bfloat16)], axis=0)
-    own_routes = lax.dynamic_slice_in_dim(expert_ids, width_index * own_rows, own_rows, 0).reshape(
-        1, own_rows * TOPK
-    )
-    owner_count = own_routes.shape[0]
-    assigns = own_routes.shape[1]
-    order_index = jnp.arange(assigns, dtype=jnp.int32)
-    matches = (own_routes[:, :, None] == own_routes[:, None, :]) & (
-        order_index[None, None, :] < order_index[None, :, None]
-    )
-    rank_in_block = jnp.sum(matches.astype(jnp.int32), axis=2)
-    slot_index = own_routes * capacity + rank_in_block
-    owner_index = jnp.arange(owner_count, dtype=jnp.int32)[:, None]
-    token_of = (width_index + owner_index) * own_rows + order_index[None, :] // TOPK
-    slot_token = (
-        jnp.full((owner_count, experts_all * capacity), block_rows, jnp.int32)
-        .at[owner_index, slot_index]
-        .set(token_of)
-    )
-    slot_single, slot_token = (slot_index, slot_token)
-    outgoing = normed_pad[slot_token].reshape(1, token_split, experts_here, capacity, model_width)
-    arrived = lax.all_to_all(outgoing, "sp", split_axis=1, concat_axis=1, tiled=True)
-    slot_batch = lax.all_gather(arrived, "tp", axis=0, tiled=True)
+    own_start = width_index * own_rows
+    own_ids = lax.dynamic_slice_in_dim(expert_ids, own_start, own_rows, 0)
+    own_routes = own_ids.reshape(own_rows * TOPK)
+    order_index = jnp.arange(own_rows * TOPK, dtype=jnp.int32)
+    matches = (own_routes[:, None] == own_routes[None, :]) & (
+        order_index[None, :] < order_index[:, None]
+    )
+    rank_in_block = jnp.sum(matches.astype(jnp.int32), axis=1)
+    slots = (own_routes * capacity + rank_in_block).reshape(own_rows, TOPK)
+    slot_count = experts_all * capacity
+    chosen = slots[:, :, None] == jnp.arange(slot_count, dtype=jnp.int32)[None, None, :]
+    sender = jnp.any(chosen, axis=1).astype(jnp.bfloat16)
+    normed_own = lax.dynamic_slice_in_dim(normed, own_start, own_rows, 0)
+    outgoing = lax.dot_general(
+        sender, normed_own, (((0,), (0,)), ((), ())), preferred_element_type=jnp.float32
+    ).astype(jnp.bfloat16)
+    outgoing = outgoing.reshape(token_split, experts_here, capacity, model_width)
+    arrived = dispatch(outgoing, token_split, width_split)
+    slot_batch = arrived.reshape(experts_here, -1, model_width)
     gate_values = jnp.einsum(
-        "osecd,edh->osech", slot_batch, expert_gate, preferred_element_type=jnp.float32
+        "erd,edh->erh", slot_batch, expert_gate, preferred_element_type=jnp.float32
     )
     up_values = jnp.einsum(
-        "osecd,edh->osech", slot_batch, expert_up, preferred_element_type=jnp.float32
+        "erd,edh->erh", slot_batch, expert_up, preferred_element_type=jnp.float32
     )
     hidden = (jax.nn.silu(gate_values) * up_values).astype(jnp.bfloat16)
     partial_value = jnp.einsum(
-        "osech,ehd->osecd", hidden, expert_down, preferred_element_type=jnp.float32
+        "erh,ehd->erd", hidden, expert_down, preferred_element_type=jnp.float32
     ).astype(jnp.bfloat16)
-    own_slots = slot_single[0]
-    summed, shared_sum = (
-        lax.psum_scatter(partial_value, "tp", scatter_dimension=0, tiled=True).astype(jnp.float32),
-        lax.psum_scatter(shared_part, "tp", scatter_dimension=0, tiled=True).astype(jnp.float32),
-    )
-    returned = lax.all_to_all(
-        summed.astype(jnp.bfloat16), "sp", split_axis=1, concat_axis=1, tiled=True
-    )
-    flat_back = returned.reshape(experts_all * capacity, model_width)
-    picked = flat_back[own_slots].astype(jnp.float32).reshape(own_rows, TOPK, model_width)
-    routed = jnp.sum(route_weights[:, :, None] * picked, axis=1)
-    mixed_own = lax.dynamic_slice_in_dim(mixed_float, width_index * own_rows, own_rows, 0)
-    return (mixed_own + shared_sum[0] + routed).astype(jnp.bfloat16)
+    returned, shared_sum = collect(
+        partial_value.reshape(arrived.shape), shared_part, token_split, width_split
+    )
+    flat_back = returned.reshape(slot_count, model_width)
+    weights = jnp.sum(jnp.where(chosen, route_weights[:, :, None], 0.0), axis=1)
+    coarse = weights.astype(jnp.bfloat16)
+    fine = (weights - coarse.astype(jnp.float32)).astype(jnp.bfloat16)
+    routed = jnp.dot(
+        jnp.concatenate([coarse, fine], axis=0), flat_back, preferred_element_type=jnp.float32
+    )
+    routed = routed[:own_rows] + routed[own_rows:]
+    mixed_own = lax.dynamic_slice_in_dim(mixed_float, own_start, own_rows, 0)
+    return (mixed_own + shared_sum + routed).astype(jnp.bfloat16)
 
 
 def solution(mesh):

time: 354 us -> 198 us (0.56)
  waiting for transfers between devices: 193 us -> 0.01 us
  Pallas kernels: 0 us -> 119 us
  blocking collectives: 52 us -> 7.74 us
  local copies, waits for them, and re-layouts: 36.7 us -> 16.9 us
  between operations: 13.4 us -> 0.34 us
  starting transfers between devices: 12.7 us -> 6.74 us
    pallas_call x0 -> x2, Pallas kernels: none -> 119 us  [the longest x1 62.1 us: collect(): pl.pallas_call(functools.partial(collect_kernel, token_split, width_split...]
    unnamed x4 -> x0, waiting for transfers between devices: 112 us -> none
    all_gather x1 -> x0, waiting for transfers between devices: 44.5 us -> none  [per_device(): slot_batch = lax.all_gather(arrived, 'tp', axis=0, tiled=True)]
    all_to_all x1 -> x0, blocking collectives: 44.4 us -> none  [per_device(): lax.all_to_all(outgoing, 'sp', split_axis=1, concat_axis=1, tiled=True)]
    all_to_all x1 -> x0, waiting for transfers between devices: 36.4 us -> none  [per_device(): lax.all_to_all(summed.astype(jnp.bfloat16), 'sp', split_axis=1, concat_ax...]
    gather x2 -> x0, local copies, waits for them, and re-layouts: 11.1 us -> none  [the longest x1 6.68 us: per_device(): normed_pad[slot_token]]
    all_to_all x1 -> x0, starting transfers between devices: 5.64 us -> none  [per_device(): lax.all_to_all(summed.astype(jnp.bfloat16), 'sp', split_axis=1, concat_ax...]
    dot_general x2 -> x4, matrix products: 17.1 us -> 20.3 us  [the longest x1 10.7 us: per_device(): jnp.einsum('erh,ehd->erd', hidden, expert_down, preferred_element_type=jn...]
  transfers between devices with their start and end apart: 6 -> 2, of which waited for: 3 -> 0; matrix products, arithmetic and copies ran while one was open for 11% -> 10% of each run, Pallas kernels for 0% -> 0%
where the time goes in v1:
time: 198 us; the launch traced here: 197 us
  Pallas kernels  119 us (60%)
  matrix products  30.8 us (16%)
  local copies, waits for them, and re-layouts  16.9 us (9%)
  other arithmetic  16 us (8%)
  blocking collectives  7.74 us (4%)
  starting transfers between devices  6.74 us (3%)
    pallas_call x1, Pallas kernels, collect(): pl.pallas_call(functools.partial(collect_kernel, token_split, width_split...  62.1 us
    pallas_call x1, Pallas kernels, dispatch(): pl.pallas_call(functools.partial(dispatch_kernel, token_split, width_spli...  56.4 us
    dot_general x1, matrix products, per_device(): jnp.einsum('erh,ehd->erd', hidden, expert_down, preferred_element_type=jn...  10.7 us
    all_gather x1, blocking collectives, per_device(): lax.all_gather(attended, 'tp', axis=1, tiled=True)  7.74 us
    dot_general x1, matrix products, per_device(): jnp.einsum('erd,edh->erh', slot_batch, expert_gate, preferred_element_typ...  5.74 us
    ppermute x1, starting transfers between devices, extended(): before = lax.ppermute(last, axis, up)  5.46 us
    unnamed x41, local copies, waits for them, and re-layouts  5.41 us
    dot_general x1, matrix products, per_device(): jnp.dot(shared_hidden, shared_down, preferred_element_type=jnp.float32)  4.72 us
  transfers between devices with their start and end apart: 2, of which 0 were waited for; matrix products, arithmetic and copies ran while one was open for 10% of the time, Pallas kernels for 0%

profile of v1, /device:TPU:0, one launch (start us, length us, event | category | flops | bytes accessed | tf_op | source)
XLA Modules:
  0.0 197.1 jit_solution(15109537095712629391)
XLA Ops:
  0.1 1.0 bitcast_convert_fusion
  2.5 1.5 copy.65
  4.0 1.2 concatenate.64
  5.8 5.5 %collective-permute-start = (bf16[128,128]{1,0:T(8,128)(2,1)}, bf16[128,128]{1,0:T(8,128)(2,1)}, u32[]{:S(2)}, u32[]{:S(2)}) collective-permute-start(bf16[128,128]{1,0:T(8,128)(2,1)} %get-tuple-element.25), channel_id=1, source_target_pairs={{0,4},{4,8},{8,12},{12,16},{16,20},{20,24},{24,28},{1,5},{5,9},{9,... | collective-permute-start | bytes 98312 | tf_op jit(solution)/shard_map/ppermute | solution.py:31
  11.3 1.3 collective-permute-start.1
  14.7 1.5 multiply_cosine_fusion.1
  17.0 0.8 bitcast_dynamic-update-slice_fusion
  18.5 0.9 convert.51
  21.0 0.9 eq.31
  21.9 0.8 convert_reduce_fusion
  22.7 1.4 reduce_sum.40
  24.1 1.4 multiply_add_fusion
  25.5 0.9 copy.80
  26.4 0.8 select_reduce_fusion
  27.9 2.3 %fusion.9 = pred[3,128,384]{1,2,0:T(8,128)(4,1)} fusion(s32[3,384]{1,0:T(4,128)S(1)} %iota_add_fusion, s32[3,128]{1,0:T(4,128)S(1)} %iota_add_fusion.1, pred[3,384]{1,0:T(4,128)(4,1)} %get-tuple-element.34, pred[3,384]{1,0:T(4,128)(4,1)} %get-tuple-element.33), kind=kLoop, calls=%fused_computation.23 | loop fusion | flops 737280 | bytes 155904 | tf_op jit(solution)/shard_map/and | solution.py:384
  30.2 0.8 fusion.30
  32.4 0.8 pad_maximum_fusion.2
  33.5 0.9 pad_maximum_fusion
  34.5 1.4 fusion.63
  36.9 7.7 %all_gather.3 = bf16[384,768]{0,1:T(8,128)(2,1)S(1)} all-gather(bf16[384,192]{0,1:T(8,128)(2,1)S(1)} %bitcast.100), channel_id=1, replica_groups=mesh['sp'=8,'tp'=4] {'tp'}, dimensions={1}, use_global_device_ids=true | all-gather | bytes 737280 | tf_op jit(solution)/shard_map/all_gather | solution.py:397
  44.7 1.8 multiply_reduce_fusion
  46.8 1.3 copy-done.2
  48.1 1.1 copy-done.1
  49.2 1.8 convolution_convert_fusion.2
  51.0 56.4 %dispatch.1 = bf16[2,4,8,24,2048]{4,3,2,1,0:T(8,128)(2,1)} custom-call(bf16[8,2,24,2048]{3,2,1,0:T(8,128)(2,1)} %bitcast.97), custom_call_target="tpu_custom_call" | custom-call | tf_op jit(solution)/shard_map/dispatch/pallas_call | solution.py:145
  107.5 2.1 %fusion.65 = f32[384,128]{1,0:T(8,128)S(1)} fusion(bf16[384,2048]{1,0:T(8,128)(2,1)} %copy-done.1, bf16[2048,128]{1,0:T(8,128)(2,1)S(1)} %copy-done.5), kind=kOutput, calls=%fused_computation.129 | convolution fusion | flops 201326592 | bytes 2293760 | tf_op jit(solution)/shard_map/dot_general | solution.py:62
  109.6 5.7 %fusion.64 = f32[2,768,256]{2,1,0:T(8,128)} fusion(bf16[2,768,2048]{2,1,0:T(8,128)(2,1)} %bitcast.94, bf16[2,2048,256]{2,1,0:T(8,128)(2,1)S(1)} %copy-done.16), kind=kOutput, calls=%fused_computation.128 | convolution fusion | flops 1610612736 | bytes 9961472 | tf_op jit(solution)/shard_map/erd,edh->erh/dot_general | solution.py:433
  115.4 10.7 %convolution_convert_fusion = bf16[2,768,2048]{2,1,0:T(8,128)(2,1)} fusion(bf16[2,256,2048]{2,1,0:T(8,128)(2,1)} %param.29, f32[2,768,256]{2,1,0:T(8,128)} %fusion.64, bf16[2,768,2048]{2,1,0:T(8,128)(2,1)} %bitcast.95, bf16[2,2048,256]{2,1,0:T(8,128)(2,1)} %param.28), kind=kOutput, calls=%fused_computation | convolution fusion | flops 3226730496 | bytes 18350080 | tf_op jit(solution)/shard_map/erh,ehd->erd/dot_general | solution.py:440
  126.1 4.7 %convolution_convert_fusion.1 = bf16[384,2048]{1,0:T(8,128)(2,1)} fusion(bf16[128,2048]{1,0:T(8,128)(2,1)} %param.24, bf16[384,2048]{1,0:T(8,128)(2,1)} %copy-done.1, bf16[2048,128]{1,0:T(8,128)(2,1)} %param.23, f32[384,128]{1,0:T(8,128)S(1)} %fusion.65), kind=kOutput, calls=%fused_computation.4 | convolution fusion | flops 403734528 | bytes 4390912 | tf_op jit(solution)/shard_map/dot_general | solution.py:409
  130.8 62.1 %collect.1 = (bf16[8,2,24,2048]{3,2,1,0:T(8,128)(2,1)}, f32[96,2048]{1,0:T(8,128)}) custom-call(bf16[2,4,8,24,2048]{4,3,2,1,0:T(8,128)(2,1)} %bitcast.93, bf16[4,96,2048]{2,1,0:T(8,128)(2,1)} %bitcast.96), custom_call_target="tpu_custom_call" | custom-call | tf_op jit(solution)/shard_map/collect/pallas_call | solution.py:296
  193.0 2.1 %fusion.25 = f32[192,2048]{1,0:T(8,128)S(1)} fusion(bf16[384,2048]{1,0:T(8,128)(2,1)} %bitcast.98, bf16[96,384]{1,0:T(8,128)(2,1)S(1)} %copy-done.6, bf16[96,384]{1,0:T(8,128)(2,1)S(1)} %copy-done.7), kind=kOutput, calls=%fused_computation.47 | convolution fusion | flops 302284800 | bytes 3293184 | tf_op jit(solution)/shard_map/dot_general | solution.py:450
  195.0 2.1 %fusion.6 = bf16[96,2048]{1,0:T(8,128)(2,1)} fusion(f32[192,2048]{1,0:T(8,128)S(1)} %fusion.25, f32[96,2048]{1,0:T(8,128)S(1)} %copy-done.4, f32[384,2048]{1,0:T(8,128)} %copy-done.2, s32[]{:T(128)S(6)} %select_n.39), kind=kLoop, calls=%fused_computation.19 | loop fusion | flops 786432 | bytes 3538948 | tf_op jit(solution)/shard_map/convert_element_type | solution.py:455
  (72 shorter events, 10.8 us)
Async XLA Ops:
  0.0 44.7 %copy-start = (bf16[768,2048]{1,0:T(8,128)(2,1)S(1)}, bf16[768,2048]{1,0:T(8,128)(2,1)}, u32[]{:S(2)}) copy-start(bf16[768,2048]{1,0:T(8,128)(2,1)} %param.20) | copy-start | bytes 9437188
  0.0 2.5 %copy-start.14 = (f32[16]{0:T(128)}, f32[16]{0:T(128)S(1)}, u32[]{:S(2)}) copy-start(f32[16]{0:T(128)S(1)} %multiply_power_fusion) | copy-start | bytes 196
  0.0 2.4 %copy-start.12 = (f32[384]{0:T(512)}, f32[384]{0:T(512)S(1)}, u32[]{:S(2)}) copy-start(f32[384]{0:T(512)S(1)} %get-tuple-element.40) | copy-start | bytes 4612
  1.3 1.2 copy-start.9
  1.3 1.2 copy-start.10
  1.3 1.2 copy-start.11
  5.8 26.6 %collective-permute-start = (bf16[128,128]{1,0:T(8,128)(2,1)}, bf16[128,128]{1,0:T(8,128)(2,1)}, u32[]{:S(2)}, u32[]{:S(2)}) collective-permute-start(bf16[128,128]{1,0:T(8,128)(2,1)} %get-tuple-element.25), channel_id=1, source_target_pairs={{0,4},{4,8},{8,12},{12,16},{16,20},{20,24},{24,28},{1,5},{5,9},{9,... | collective-permute-start | bytes 98312 | tf_op jit(solution)/shard_map/ppermute | solution.py:31
  11.3 21.2 %collective-permute-start.1 = (bf16[128,128]{1,0:T(8,128)(2,1)}, bf16[128,128]{1,0:T(8,128)(2,1)}, u32[]{:S(2)}, u32[]{:S(2)}) collective-permute-start(bf16[128,128]{1,0:T(8,128)(2,1)} %get-tuple-element.26), channel_id=1, source_target_pairs={{4,0},{8,4},{12,8},{16,12},{20,16},{24,20},{28,24},{5,1},{9,5},{13... | collective-permute-start | bytes 98312 | tf_op jit(solution)/shard_map/ppermute | solution.py:32
  17.9 0.6 copy-start.8
  33.2 2.7 %copy-start.15 = (f32[3]{0:T(128)S(1)}, f32[3]{0:T(128)}, u32[]{:S(2)}) copy-start(f32[3]{0:T(128)} %param.18) | copy-start | bytes 40
  36.3 8.4 %copy-start.3 = (bf16[384,2048]{1,0:T(8,128)(2,1)S(1)}, bf16[384,2048]{1,0:T(8,128)(2,1)}, u32[]{:S(2)}) copy-start(bf16[384,2048]{1,0:T(8,128)(2,1)} %param.19) | copy-start | bytes 4718596
  44.7 1.8 copy-start.13
  46.5 1.6 copy-start.2
  48.1 1.1 copy-start.1
  51.0 56.4 %copy-start.5 = (bf16[2048,128]{1,0:T(8,128)(2,1)S(1)}, bf16[2048,128]{1,0:T(8,128)(2,1)}, u32[]{:S(2)}) copy-start(bf16[2048,128]{1,0:T(8,128)(2,1)} %param.22) | copy-start | bytes 1572868
  107.5 2.1 %copy-start.16 = (bf16[2,2048,256]{2,1,0:T(8,128)(2,1)S(1)}, bf16[2,2048,256]{2,1,0:T(8,128)(2,1)}, u32[]{:S(2)}) copy-start(bf16[2,2048,256]{2,1,0:T(8,128)(2,1)} %param.27) | copy-start | bytes 6291460
  130.8 62.2 %copy-start.6 = (bf16[96,384]{1,0:T(8,128)(2,1)S(1)}, bf16[96,384]{1,0:T(8,128)(2,1)}, u32[]{:S(2)}) copy-start(bf16[96,384]{1,0:T(8,128)(2,1)} %get-tuple-element.9) | copy-start | bytes 221188
  130.8 62.2 %copy-start.7 = (bf16[96,384]{1,0:T(8,128)(2,1)S(1)}, bf16[96,384]{1,0:T(8,128)(2,1)}, u32[]{:S(2)}) copy-start(bf16[96,384]{1,0:T(8,128)(2,1)} %get-tuple-element.10) | copy-start | bytes 221188
  192.9 2.1 %copy-start.4 = (f32[96,2048]{1,0:T(8,128)S(1)}, f32[96,2048]{1,0:T(8,128)}, u32[]{:S(2)}) copy-start(f32[96,2048]{1,0:T(8,128)} %get-tuple-element.7) | copy-start | bytes 2359300

commit v2 on v1

--- a/solution.py
+++ b/solution.py
@@ -1,5 +1,6 @@
 import jax
 import jax.numpy as jnp
+import numpy as np
 from jax import lax
 from jax.experimental import pallas as pl
 from jax.experimental.pallas import tpu as pltpu
@@ -34,28 +35,110 @@
     return x
 
 
-def rotary_turn(values, places, turn_sign):
-    halfway = values.shape[-1] // 2
+def rotary_turn(values, places):
+    heads = values.shape[1] // HEAD_DIM
+    halfway = HEAD_DIM // 2
     quarter = halfway // 2
+    column = np.arange(HEAD_DIM)
+    swap = np.zeros((HEAD_DIM, HEAD_DIM), np.float32)
+    for d in range(HEAD_DIM):
+        if d % halfway < quarter:
+            swap[d + quarter, d] = -1.0
+        else:
+            swap[d - quarter, d] = 1.0
+    swap = jnp.asarray(np.kron(np.eye(heads, dtype=np.float32), swap), jnp.bfloat16)
     spectrum = ROPE_BASE ** (-jnp.arange(0, halfway, 2, dtype=jnp.float32) / halfway)
-
-    def rotate_by(segment, offsets_at):
-        angles = turn_sign * offsets_at.astype(jnp.float32)[:, None] * spectrum[None, :]
-        cosine = jnp.cos(angles)[:, None, :]
-        sine_part = jnp.sin(angles)[:, None, :]
-        former = segment[..., :quarter]
-        latter = segment[..., quarter:]
-        return jnp.concatenate(
-            [former * cosine - latter * sine_part, former * sine_part + latter * cosine], axis=-1
-        )
-
-    return jnp.concatenate(
-        [
-            rotate_by(values[..., :halfway], places // GRID_W),
-            rotate_by(values[..., halfway:], places % GRID_W),
-        ],
-        axis=-1,
-    )
+    spectrum = jnp.tile(spectrum, values.shape[1] // quarter)
+    first_half = jnp.asarray(np.tile(column < halfway, heads))
+    offsets = jnp.where(
+        first_half[None, :], (places // GRID_W)[:, None], (places % GRID_W)[:, None]
+    )
+    angles = offsets.astype(jnp.float32) * spectrum[None, :]
+    swapped = jnp.dot(values, swap, preferred_element_type=jnp.float32)
+    return (values.astype(jnp.float32) * jnp.cos(angles) + swapped * jnp.sin(angles)).astype(
+        jnp.bfloat16
+    )
+
+
+def attend_kernel(key_heads, total_rows, first_ref, sink_ref, q_ref, kv_ref, out_ref):
+    first = first_ref[0]
+    heads = q_ref.shape[1] // HEAD_DIM
+    group = heads // key_heads
+    shape = (WINDOW, 3 * WINDOW)
+    row = lax.broadcasted_iota(jnp.int32, shape, 0)
+    column = lax.broadcasted_iota(jnp.int32, shape, 1) - WINDOW
+    near = jnp.abs(row - column) <= WINDOW
+    for block in range(q_ref.shape[0] // WINDOW):
+        start = block * WINDOW
+        key_at = column + (first + start)
+        allowed = near & (key_at >= 0) & (key_at < total_rows)
+        for kh in range(key_heads):
+            span = slice(start, start + 3 * WINDOW)
+            key = kv_ref[span, kh * HEAD_DIM : (kh + 1) * HEAD_DIM]
+            value = kv_ref[span, (key_heads + kh) * HEAD_DIM : (key_heads + kh + 1) * HEAD_DIM]
+            for h in range(kh * group, (kh + 1) * group):
+                query = q_ref[start : start + WINDOW, h * HEAD_DIM : (h + 1) * HEAD_DIM]
+                scores = lax.dot_general(
+                    query, key, (((1,), (1,)), ((), ())), preferred_element_type=jnp.float32
+                ) * HEAD_DIM ** (-0.5)
+                scores = jnp.where(allowed, scores, NEG_LARGE)
+                sink = sink_ref[h]
+                highest = jnp.maximum(jnp.max(scores, axis=1, keepdims=True), sink)
+                lifted = jnp.exp(scores - highest)
+                below = jnp.sum(lifted, axis=1, keepdims=True) + jnp.exp(sink - highest)
+                chances = (lifted / below).astype(jnp.bfloat16)
+                result = jnp.dot(chances, value, preferred_element_type=jnp.float32)
+                out_ref[start : start + WINDOW, h * HEAD_DIM : (h + 1) * HEAD_DIM] = result.astype(
+                    jnp.bfloat16
+                )
+
+
+def attend(first, sinks, turned, widened, key_heads, total_rows):
+    smem = pl.BlockSpec(memory_space=pltpu.SMEM)
+    return pl.pallas_call(
+        functools.partial(attend_kernel, key_heads, total_rows),
+        out_shape=jax.ShapeDtypeStruct(turned.shape, jnp.bfloat16),
+        in_specs=[smem, smem, VMEM, VMEM],
+        out_specs=VMEM,
+        name="attend",
+    )(first.reshape(1), sinks, turned, widened)
+
+
+def routes_kernel(capacity, ids_ref, ids_row_ref, weights_ref, sender_ref, weigh_ref):
+    own, slot_count = sender_ref.shape
+    earlier = lax.broadcasted_iota(jnp.int32, (own, own), 1) < lax.broadcasted_iota(
+        jnp.int32, (own, own), 0
+    )
+    slot_of = lax.broadcasted_iota(jnp.int32, (own, slot_count), 1)
+    taken = jnp.zeros((own, slot_count), jnp.float32)
+    weigh = jnp.zeros((own, slot_count), jnp.float32)
+    for k in range(TOPK):
+        mine = ids_ref[:, k : k + 1]
+        rank = jnp.zeros((own, 1), jnp.int32)
+        for other in range(TOPK):
+            same = (ids_row_ref[other : other + 1, :] == mine) & earlier
+            rank = rank + jnp.sum(same.astype(jnp.int32), axis=1, keepdims=True)
+        chosen = slot_of == mine * capacity + rank
+        taken = jnp.where(chosen, 1.0, taken)
+        weigh = jnp.where(chosen, weights_ref[:, k : k + 1], weigh)
+    sender_ref[...] = taken.astype(jnp.bfloat16)
+    coarse = weigh.astype(jnp.bfloat16)
+    weigh_ref[:own, :] = coarse
+    weigh_ref[own:, :] = (weigh - coarse.astype(jnp.float32)).astype(jnp.bfloat16)
+
+
+def routes(own_ids, weights, capacity, slot_count):
+    own = own_ids.shape[0]
+    return pl.pallas_call(
+        functools.partial(routes_kernel, capacity),
+        out_shape=(
+            jax.ShapeDtypeStruct((own, slot_count), jnp.bfloat16),
+            jax.ShapeDtypeStruct((2 * own, slot_count), jnp.bfloat16),
+        ),
+        in_specs=[VMEM] * 3,
+        out_specs=(VMEM, VMEM),
+        name="routes",
+    )(own_ids, own_ids.T, weights)
 
 
 def gated_hidden(gathered_rows, gate_weight, up_weight):
@@ -86,7 +169,20 @@
     pl.semaphore_wait(barrier, token_split + 1)
 
 
-def dispatch_kernel(token_split, width_split, rows_ref, out_ref, local_sem, send, recv):
+def dispatch_kernel(
+    token_split,
+    width_split,
+    rows_ref,
+    normed_ref,
+    gate_ref,
+    up_ref,
+    down_ref,
+    out_ref,
+    shared_ref,
+    local_sem,
+    send,
+    recv,
+):
     sp_at, tp_at, pair, cross = places_of(token_split, width_split)
     greet(token_split, sp_at, tp_at, pair, cross)
 
@@ -124,6 +220,14 @@
         passed(1, i, tp_at, cross).start()
         passed(2, i, tp_at, pair).start()
 
+    own_rows = shared_ref.shape[1]
+    for block in range(width_split):
+        here = normed_ref[block * own_rows : (block + 1) * own_rows, :]
+        hidden = gated_hidden(here, gate_ref[...], up_ref[...])
+        shared_ref[block] = jnp.dot(
+            hidden, down_ref[...], preferred_element_type=jnp.float32
+        ).astype(shared_ref.dtype)
+
     @pl.loop(0, token_split)
     def _(i):
         passed(1, i, tp_at, cross).wait_recv()
@@ -140,15 +244,18 @@
         along(i).wait_send()
 
 
-def dispatch(rows, token_split, width_split):
+def dispatch(rows, normed, gate, up, down, token_split, width_split):
     _, experts, cap, width = rows.shape
     return pl.pallas_call(
         functools.partial(dispatch_kernel, token_split, width_split),
-        out_shape=jax.ShapeDtypeStruct(
-            (experts, width_split, token_split, cap, width), rows.dtype
+        out_shape=(
+            jax.ShapeDtypeStruct((experts, width_split, token_split, cap, width), rows.dtype),
+            jax.ShapeDtypeStruct(
+                (width_split, normed.shape[0] // width_split, width), rows.dtype
+            ),
         ),
-        in_specs=[VMEM],
-        out_specs=VMEM,
+        in_specs=[VMEM] * 5,
+        out_specs=(VMEM, VMEM),
         scratch_shapes=[
             pltpu.SemaphoreType.DMA,
             pltpu.SemaphoreType.DMA((4, token_split)),
@@ -158,7 +265,7 @@
             collective_id=1, has_side_effects=True, vmem_limit_bytes=VMEM_LIMIT
         ),
         name="dispatch",
-    )(rows)
+    )(rows, normed, gate, up, down)
 
 
 def collect_kernel(
@@ -344,54 +451,16 @@
     width_index = lax.axis_index("tp")
     key_heads = keys.shape[1] // HEAD_DIM
     heads_local = queries.shape[1] // HEAD_DIM
-    group_size = heads_local // key_heads
     first_row = lax.axis_index("sp") * block_rows
     total_rows = token_split * block_rows
     places = first_row + jnp.arange(block_rows, dtype=jnp.int32)
-    turned_queries = rotary_turn(
-        queries.astype(jnp.float32).reshape(block_rows, heads_local, HEAD_DIM), places, 1.0
-    ).astype(jnp.bfloat16)
-    turned_keys = rotary_turn(
-        keys.astype(jnp.float32).reshape(block_rows, key_heads, HEAD_DIM), places, 1.0
-    ).astype(jnp.bfloat16)
-    joined = jnp.concatenate(
-        [turned_keys.reshape(block_rows, key_heads * HEAD_DIM), values], axis=1
-    )
+    turned = rotary_turn(jnp.concatenate([queries, keys], axis=1), places)
+    query_width = heads_local * HEAD_DIM
+    joined = jnp.concatenate([turned[:, query_width:], values], axis=1)
     widened = extended(joined, (("sp", 0),), WINDOW)
-    blocks = block_rows // WINDOW
-    windows = jnp.concatenate(
-        [
-            widened[shift_index * WINDOW : shift_index * WINDOW + blocks * WINDOW].reshape(
-                blocks, WINDOW, -1
-            )
-            for shift_index in range(3)
-        ],
-        axis=1,
-    )
-    key_win = windows[..., : key_heads * HEAD_DIM].reshape(blocks, 3 * WINDOW, key_heads, HEAD_DIM)
-    value_win = windows[..., key_heads * HEAD_DIM :].reshape(
-        blocks, 3 * WINDOW, key_heads, HEAD_DIM
-    )
-    query_blocks = turned_queries.reshape(blocks, WINDOW, key_heads, group_size, HEAD_DIM)
-    scores = jnp.einsum(
-        "bqkgd,bmkd->bkgqm", query_blocks, key_win, preferred_element_type=jnp.float32
-    ) * HEAD_DIM ** (-0.5)
-    block_first = first_row + jnp.arange(blocks, dtype=jnp.int32) * WINDOW
-    query_at = block_first[:, None, None] + jnp.arange(WINDOW, dtype=jnp.int32)[None, :, None]
-    key_at = (
-        block_first[:, None, None] - WINDOW + jnp.arange(3 * WINDOW, dtype=jnp.int32)[None, None, :]
-    )
-    allowed = (jnp.abs(query_at - key_at) <= WINDOW) & (key_at >= 0) & (key_at < total_rows)
-    scores = jnp.where(allowed[:, None, None], scores, NEG_LARGE)
-    sink_logit = sinks.reshape(key_heads, group_size)[None, :, :, None, None]
-    highest = jnp.maximum(jnp.max(scores, axis=-1, keepdims=True), sink_logit)
-    lifted = jnp.exp(scores - highest)
-    denominator = jnp.sum(lifted, axis=-1, keepdims=True) + jnp.exp(sink_logit - highest)
-    probabilities = (lifted / denominator).astype(jnp.bfloat16)
-    attended = jnp.einsum(
-        "bkgqm,bmkd->bqkgd", probabilities, value_win, preferred_element_type=jnp.float32
-    )
-    attended = attended.astype(jnp.bfloat16).reshape(block_rows, heads_local * HEAD_DIM)
+    attended = attend(
+        first_row, sinks, turned[:, :query_width], widened, key_heads, total_rows
+    )
     model_width = out_weight.shape[1]
     projected = jnp.dot(
         lax.all_gather(attended, "tp", axis=1, tiled=True),
@@ -405,30 +474,21 @@
     )
     normed = (mixed_float * scale_rows * norm_gain).astype(jnp.bfloat16)
     own_rows = block_rows // width_split
-    shared_hidden = gated_hidden(normed, shared_gate, shared_up)
-    shared_part = jnp.dot(shared_hidden, shared_down, preferred_element_type=jnp.float32)
-    shared_part = shared_part.astype(jnp.bfloat16).reshape(width_split, own_rows, model_width)
     experts_here = expert_gate.shape[0]
     experts_all = experts_here * token_split
     capacity = max(2, 2 * own_rows * TOPK // experts_all)
     own_start = width_index * own_rows
     own_ids = lax.dynamic_slice_in_dim(expert_ids, own_start, own_rows, 0)
-    own_routes = own_ids.reshape(own_rows * TOPK)
-    order_index = jnp.arange(own_rows * TOPK, dtype=jnp.int32)
-    matches = (own_routes[:, None] == own_routes[None, :]) & (
-        order_index[None, :] < order_index[:, None]
-    )
-    rank_in_block = jnp.sum(matches.astype(jnp.int32), axis=1)
-    slots = (own_routes * capacity + rank_in_block).reshape(own_rows, TOPK)
     slot_count = experts_all * capacity
-    chosen = slots[:, :, None] == jnp.arange(slot_count, dtype=jnp.int32)[None, None, :]
-    sender = jnp.any(chosen, axis=1).astype(jnp.bfloat16)
+    sender, weigh = routes(own_ids, route_weights, capacity, slot_count)
     normed_own = lax.dynamic_slice_in_dim(normed, own_start, own_rows, 0)
     outgoing = lax.dot_general(
         sender, normed_own, (((0,), (0,)), ((), ())), preferred_element_type=jnp.float32
     ).astype(jnp.bfloat16)
     outgoing = outgoing.reshape(token_split, experts_here, capacity, model_width)
-    arrived = dispatch(outgoing, token_split, width_split)
+    arrived, shared_part = dispatch(
+        outgoing, normed, shared_gate, shared_up, shared_down, token_split, width_split
+    )
     slot_batch = arrived.reshape(experts_here, -1, model_width)
     gate_values = jnp.einsum(
         "erd,edh->erh", slot_batch, expert_gate, preferred_element_type=jnp.float32
@@ -444,12 +504,7 @@
         partial_value.reshape(arrived.shape), shared_part, token_split, width_split
     )
     flat_back = returned.reshape(slot_count, model_width)
-    weights = jnp.sum(jnp.where(chosen, route_weights[:, :, None], 0.0), axis=1)
-    coarse = weights.astype(jnp.bfloat16)
-    fine = (weights - coarse.astype(jnp.float32)).astype(jnp.bfloat16)
-    routed = jnp.dot(
-        jnp.concatenate([coarse, fine], axis=0), flat_back, preferred_element_type=jnp.float32
-    )
+    routed = jnp.dot(weigh, flat_back, preferred_element_type=jnp.float32)
     routed = routed[:own_rows] + routed[own_rows:]
     mixed_own = lax.dynamic_slice_in_dim(mixed_float, own_start, own_rows, 0)
     return (mixed_own + shared_sum + routed).astype(jnp.bfloat16)

time: 198 us -> 185 us (0.934)
  other arithmetic: 16 us -> 4.71 us
  Pallas kernels: 119 us -> 126 us
  local copies, waits for them, and re-layouts: 16.9 us -> 10.1 us
  matrix products: 30.8 us -> 28 us
    pallas_call x0 -> x2, Pallas kernels: none -> 7 us  [the longest x1 5.02 us: attend(): pl.pallas_call(functools.partial(attend_kernel, key_heads, total_rows), o...]
    concatenate x14 -> x0, local copies, waits for them, and re-layouts: 6.54 us -> none  [the longest x12 4.57 us: rotary_turn(): jnp.concatenate([rotate_by(values[..., :halfway], places // GRID_W), rota...]
    dot_general x5 -> x3, matrix products: 10.8 us -> 5.94 us  [the longest x2 3.89 us: rotary_turn(): swapped = jnp.dot(values, swap, preferred_element_type=jnp.float32)]
    and x1 -> x0, other arithmetic: 2.34 us -> none  [per_device(): (jnp.abs(query_at - key_at) <= WINDOW) & (key_at >= 0)]
    unnamed x41 -> x24, local copies, waits for them, and re-layouts: 5.41 us -> 6.84 us
  transfers between devices with their start and end apart: 2 -> 2, of which waited for: 0 -> 1; matrix products, arithmetic and copies ran while one was open for 10% -> 1% of each run, Pallas kernels for 0% -> 1%
where the time goes in v2:
time: 185 us; the launch traced here: 184 us
  Pallas kernels  126 us (68%)
  matrix products  28 us (15%)
  local copies, waits for them, and re-layouts  10.1 us (5%)
  blocking collectives  7.73 us (4%)
  starting transfers between devices  6.77 us (4%)
  other arithmetic  4.71 us (3%)
    pallas_call x1, Pallas kernels, collect(): pl.pallas_call(functools.partial(collect_kernel, token_split, width_split...  62.1 us
    pallas_call x1, Pallas kernels, dispatch(): pl.pallas_call(functools.partial(dispatch_kernel, token_split, width_spli...  57.1 us
    dot_general x1, matrix products, per_device(): jnp.einsum('erh,ehd->erd', hidden, expert_down, preferred_element_type=jn...  10.7 us
    all_gather x1, blocking collectives, per_device(): lax.all_gather(attended, 'tp', axis=1, tiled=True)  7.73 us
    unnamed x24, local copies, waits for them, and re-layouts  6.84 us
    dot_general x1, matrix products, per_device(): jnp.einsum('erd,edh->erh', slot_batch, expert_gate, preferred_element_typ...  6.38 us
    ppermute x1, starting transfers between devices, extended(): before = lax.ppermute(last, axis, up)  5.49 us
    pallas_call x1, Pallas kernels, attend(): pl.pallas_call(functools.partial(attend_kernel, key_heads, total_rows), o...  5.02 us
  transfers between devices with their start and end apart: 2, of which 1 were waited for; matrix products, arithmetic and copies ran while one was open for 1% of the time, Pallas kernels for 1%

profile of v2, /device:TPU:0, one launch (start us, length us, event | category | flops | bytes accessed | tf_op | source)
XLA Modules:
  0.0 184.4 jit_solution(4368682379730596880)
XLA Ops:
  0.1 0.7 mul.57
  0.7 1.0 copy.29
  1.7 0.9 copy.26
  2.6 1.7 copy.25
  4.4 1.2 fusion.14
  5.6 2.7 %fusion.4 = bf16[384,256]{1,0:T(8,128)(2,1)S(1)} fusion(f32[256,384]{0,1:T(8,128)S(1)} %fusion.14, bf16[64,256]{1,0:T(8,128)(2,1)} %constant.70, bf16[384,64]{0,1:T(8,128)(2,1)} %param.18, bf16[384,64]{1,0:T(8,128)(2,1)S(1)} %copy.26, bf16[384,192]{1,0:T(8,128)(2,1)} %copy.25, f32[256]{0:T(256)} %mul.57, s32[384]{0:T(512)S(1)} %get-tuple-element.21, ...), kind=kOutput, calls=%fused_computation.11 | convolution fusion | flops 13762560 | bytes 872704 | tf_op jit(solution)/shard_map/dot_general | solution.py:57
  8.3 0.0 copy-start.4
  8.3 0.1 slice.27
  8.4 0.7 pad_maximum_fusion.2
  9.1 5.5 %collective-permute-start = (bf16[128,128]{1,0:T(8,128)(2,1)}, bf16[128,128]{1,0:T(8,128)(2,1)}, u32[]{:S(2)}, u32[]{:S(2)}) collective-permute-start(bf16[128,128]{1,0:T(8,128)(2,1)} %get-tuple-element.17), channel_id=1, source_target_pairs={{0,4},{4,8},{8,12},{12,16},{16,20},{20,24},{24,28},{1,5},{5,9},{9,... | collective-permute-start | bytes 98312 | tf_op jit(solution)/shard_map/ppermute | solution.py:32
  14.6 1.3 collective-permute-start.1
  15.9 0.6 fusion.31.ids_row_ref
  16.5 0.1 constant_dynamic-slice_fusion
  16.6 0.7 copy.31.ids_ref
  17.3 0.7 copy.32.weights_ref
  18.0 2.0 %routes.1 = (bf16[96,384]{1,0:T(8,128)(2,1)}, bf16[192,384]{1,0:T(8,128)(2,1)}) custom-call(s32[96,2]{1,0:T(8,128)} %copy.31.ids_ref, s32[2,96]{1,0:T(2,128)} %fusion.31.ids_row_ref, f32[96,2]{1,0:T(8,128)} %copy.32.weights_ref), custom_call_target="tpu_custom_call" | custom-call | tf_op jit(solution)/shard_map/routes/pallas_call | solution.py:132
  20.0 0.7 collective-permute-done.1
  20.7 1.5 pad_maximum_fusion.kv_ref
  22.2 5.0 %attend.1 = bf16[384,192]{1,0:T(8,128)(2,1)} custom-call(s32[1]{0:T(128)} %bitcast.first_ref, f32[3]{0:T(128)} %sink_ref.1, bf16[384,192]{1,0:T(8,128)(2,1)} %bitcast.33, bf16[640,128]{1,0:T(8,128)(2,1)} %pad_maximum_fusion.kv_ref), custom_call_target="tpu_custom_call" | custom-call | tf_op jit(solution)/shard_map/attend/pallas_call | solution.py:98
  27.3 1.1 copy.30
  28.3 7.7 %all_gather.3 = bf16[384,768]{0,1:T(8,128)(2,1)S(1)} all-gather(bf16[384,192]{0,1:T(8,128)(2,1)S(1)} %copy.30), channel_id=1, replica_groups=mesh['sp'=8,'tp'=4] {'tp'}, dimensions={1}, use_global_device_ids=true | all-gather | bytes 737280 | tf_op jit(solution)/shard_map/all_gather | solution.py:466
  36.1 3.2 %multiply_reduce_fusion = (f32[384]{0:T(512)S(1)}, f32[384,2048]{1,0:T(8,128)S(1)}) fusion(bf16[384,768]{0,1:T(8,128)(2,1)S(1)} %all_gather.3, bf16[768,2048]{1,0:T(8,128)(2,1)S(1)} %copy-done, bf16[384,2048]{1,0:T(8,128)(2,1)} %param.21), kind=kOutput, calls=%fused_computation.2 | convolution fusion | flops 1212677760 | bytes 8455680 | tf_op jit(solution)/shard_map/dot_general | solution.py:465
  39.3 0.3 multiply_convert_fusion.normed_ref
  39.6 1.3 copy-done.1
  40.9 1.1 copy-done.2
  42.0 1.8 convolution_convert_fusion.1
  43.9 57.1 %dispatch.1 = (bf16[2,4,8,24,2048]{4,3,2,1,0:T(8,128)(2,1)}, bf16[4,96,2048]{2,1,0:T(8,128)(2,1)}) custom-call(bf16[8,2,24,2048]{3,2,1,0:T(8,128)(2,1)} %bitcast.30, bf16[384,2048]{1,0:T(8,128)(2,1)} %copy-done.2, bf16[2048,128]{1,0:T(8,128)(2,1)} %gate_ref.1, bf16[2048,128]{1,0:T(8,128)(2,1)} %up_ref.1, bf16[128,2048]{1,0:T(8,128)(2,1)} %down_ref.1), custom_call_target="tpu_custom_call" | custom-call | tf_op jit(solution)/shard_map/dispatch/pallas_call | solution.py:249
  101.0 6.4 %fusion.15 = f32[2,768,256]{2,1,0:T(8,128)} fusion(bf16[2,768,2048]{2,1,0:T(8,128)(2,1)} %bitcast.34, bf16[2,2048,256]{2,1,0:T(8,128)(2,1)} %param.29), kind=kOutput, calls=%fused_computation.36 | convolution fusion | flops 1610612736 | bytes 9961472 | tf_op jit(solution)/shard_map/erd,edh->erh/dot_general | solution.py:493
  107.3 10.7 %convolution_convert_fusion = bf16[2,768,2048]{2,1,0:T(8,128)(2,1)} fusion(bf16[2,256,2048]{2,1,0:T(8,128)(2,1)} %param.31, f32[2,768,256]{2,1,0:T(8,128)} %fusion.15, bf16[2,768,2048]{2,1,0:T(8,128)(2,1)} %bitcast.35, bf16[2,2048,256]{2,1,0:T(8,128)(2,1)} %param.30), kind=kOutput, calls=%fused_computation | convolution fusion | flops 3226730496 | bytes 18350080 | tf_op jit(solution)/shard_map/erh,ehd->erd/dot_general | solution.py:500
  118.0 62.1 %collect.1 = (bf16[8,2,24,2048]{3,2,1,0:T(8,128)(2,1)}, f32[96,2048]{1,0:T(8,128)}) custom-call(bf16[2,4,8,24,2048]{4,3,2,1,0:T(8,128)(2,1)} %bitcast.31, bf16[4,96,2048]{2,1,0:T(8,128)(2,1)} %get-tuple-element.13.shared_ref), custom_call_target="tpu_custom_call" | custom-call | tf_op jit(solution)/shard_map/collect/pallas_call | solution.py:403
  180.2 2.0 %fusion.16 = f32[192,2048]{1,0:T(8,128)S(1)} fusion(bf16[192,384]{1,0:T(8,128)(2,1)S(1)} %copy-done.5, bf16[384,2048]{1,0:T(8,128)(2,1)} %bitcast.32), kind=kOutput, calls=%fused_computation.37 | convolution fusion | flops 301989888 | bytes 3293184 | tf_op jit(solution)/shard_map/dot_general | solution.py:507
  182.3 2.1 %fusion.6 = bf16[96,2048]{1,0:T(8,128)(2,1)} fusion(f32[192,2048]{1,0:T(8,128)S(1)} %fusion.16, f32[96,2048]{1,0:T(8,128)S(1)} %copy-done.3, f32[384,2048]{1,0:T(8,128)} %copy-done.1, s32[]{:T(128)S(6)} %select_n.32), kind=kLoop, calls=%fused_computation.14 | loop fusion | flops 786432 | bytes 3538948 | tf_op jit(solution)/shard_map/convert_element_type | solution.py:510
  (22 shorter events, 0.1 us)
Async XLA Ops:
  0.0 36.1 %copy-start = (bf16[768,2048]{1,0:T(8,128)(2,1)S(1)}, bf16[768,2048]{1,0:T(8,128)(2,1)}, u32[]{:S(2)}) copy-start(bf16[768,2048]{1,0:T(8,128)(2,1)} %param.22) | copy-start | bytes 9437188
  0.0 15.9 %copy-start.8 = (s32[384,2]{0,1:T(2,128)S(1)}, s32[384,2]{0,1:T(2,128)}, u32[]{:S(2)}) copy-start(s32[384,2]{0,1:T(2,128)} %param.27) | copy-start | bytes 9220
  0.0 17.3 %copy-start.9 = (f32[96,2]{0,1:T(2,128)S(1)}, f32[96,2]{0,1:T(2,128)}, u32[]{:S(2)}) copy-start(f32[96,2]{0,1:T(2,128)} %param.28) | copy-start | bytes 2308
  8.3 14.0 %copy-start.4 = (bf16[384,256]{1,0:T(8,128)(2,1)}, bf16[384,256]{1,0:T(8,128)(2,1)S(1)}, u32[]{:S(2)}) copy-start(bf16[384,256]{1,0:T(8,128)(2,1)S(1)} %fusion.4) | copy-start | bytes 589828
  9.1 10.9 %collective-permute-start = (bf16[128,128]{1,0:T(8,128)(2,1)}, bf16[128,128]{1,0:T(8,128)(2,1)}, u32[]{:S(2)}, u32[]{:S(2)}) collective-permute-start(bf16[128,128]{1,0:T(8,128)(2,1)} %get-tuple-element.17), channel_id=1, source_target_pairs={{0,4},{4,8},{8,12},{12,16},{16,20},{20,24},{24,28},{1,5},{5,9},{9,... | collective-permute-start | bytes 98312 | tf_op jit(solution)/shard_map/ppermute | solution.py:32
  14.6 6.1 %collective-permute-start.1 = (bf16[128,128]{1,0:T(8,128)(2,1)}, bf16[128,128]{1,0:T(8,128)(2,1)}, u32[]{:S(2)}, u32[]{:S(2)}) collective-permute-start(bf16[128,128]{1,0:T(8,128)(2,1)} %get-tuple-element.18), channel_id=1, source_target_pairs={{4,0},{8,4},{12,8},{16,12},{20,16},{24,20},{28,24},{5,1},{9,5},{13... | collective-permute-start | bytes 98312 | tf_op jit(solution)/shard_map/ppermute | solution.py:33
  36.1 3.2 %copy-start.7 = (f32[2048]{0:T(1024)S(1)}, f32[2048]{0:T(1024)}, u32[]{:S(2)}) copy-start(f32[2048]{0:T(1024)} %param.23) | copy-start | bytes 24580
  39.2 1.7 copy-start.1
  39.3 2.8 %copy-start.6 = (bf16[96,384]{1,0:T(8,128)(2,1)S(1)}, bf16[96,384]{1,0:T(8,128)(2,1)}, u32[]{:S(2)}) copy-start(bf16[96,384]{1,0:T(8,128)(2,1)} %get-tuple-element.11) | copy-start | bytes 221188
  40.9 1.1 copy-start.2
  118.0 62.2 %copy-start.5 = (bf16[192,384]{1,0:T(8,128)(2,1)S(1)}, bf16[192,384]{1,0:T(8,128)(2,1)}, u32[]{:S(2)}) copy-start(bf16[192,384]{1,0:T(8,128)(2,1)} %get-tuple-element.15) | copy-start | bytes 442372
  180.2 2.1 %copy-start.3 = (f32[96,2048]{1,0:T(8,128)S(1)}, f32[96,2048]{1,0:T(8,128)}, u32[]{:S(2)}) copy-start(f32[96,2048]{1,0:T(8,128)} %get-tuple-element.14) | copy-start | bytes 2359300
